TPU v7x, 512 devices: a whole 4x8x8 slice. The times are simulated.
512 devices in a mesh: fs: 64 (over z, y), tp: 8 (over x, core).
Axes of the slice: x: 4, y: 8, z: 8, core: 2. Of those that a mesh axis runs over, the one named last changes fastest.
Arguments:
- inputs: bfloat16 [32768, 2048], P('fs', 'tp'), may hold values from -6 to 6
- value_cotangent: bfloat16 [32768, 2048], P('fs', 'tp'), may hold values from -6 to 6
- first_map: bfloat16 [32768, 2048], P('fs', 'tp'), may hold values from -6 to 6
- second_map: bfloat16 [32768, 2048], P('fs', 'tp'), may hold values from -6 to 6
- lambdas: float32 [16], P('tp'), may hold values from 0.3 to 0.8
- head_gain: float32 [128], replicated, may hold values from 0.1 to 1.9
- output_cotangent: bfloat16 [32768, 2048], P('fs', 'tp'), may hold values from -6 to 6
- value_factor: bfloat16 [2048, 256], replicated, may hold values from -0.125 to 0.125
- output_factor: bfloat16 [2048, 256], replicated, may hold values from -0.125 to 0.125
- value_weight: float32 [2048, 2048], P('fs', 'tp'), may hold values from -0.125 to 0.125
- output_weight: float32 [2048, 2048], P('tp', 'fs'), may hold values from -0.125 to 0.125
- value_moment: float32 [256, 2048], P('fs', 'tp'), may hold values from -6 to 6
- value_second: float32 [256, 2048], P('fs', 'tp'), may hold values from 0.25 to 4
- output_moment: float32 [256, 2048], P('fs', 'tp'), may hold values from -6 to 6
- output_second: float32 [256, 2048], P('fs', 'tp'), may hold values from 0.25 to 4
Outputs:
- value_master: float32 [2048, 2048], P('fs', 'tp')
- output_master: float32 [2048, 2048], P('tp', 'fs')
- value_moment_new: float32 [256, 2048], P('fs', 'tp')
- value_second_new: float32 [256, 2048], P('fs', 'tp')
- output_moment_new: float32 [256, 2048], P('fs', 'tp')
- output_second_new: float32 [256, 2048], P('fs', 'tp')
- value_copy: bfloat16 [2048, 2048], P(None, 'tp')
- output_copy: bfloat16 [2048, 2048], P('tp')
All inputs are finite; a program needn't handle non-finite values.
Results may differ from a plain program's by a relative error of at most 0.0027.
Values may be sent and summed in bfloat16 or wider, within the bound.
No kernel may reach another device: no remote copies, remote signals or barrier semaphores. Data moves between devices by JAX's collectives and lax.ppermute only.
A program may use at most 64 MiB of HBM per device.

v0:
```python
import math
import jax
import jax.numpy as jnp
from jax import lax
from jax.sharding import PartitionSpec as P


def side_by_side(arrays, axis, dim, along):
    ends, at = ([], 0)
    for a in arrays[:-1]:
        at += a.shape[along]
        ends.append(at)
    both = jnp.concatenate(arrays, axis=along)
    return tuple(jnp.split(lax.all_gather(both, axis, axis=dim, tiled=True), ends, axis=along))


def cut_along(x, dim, size):
    before, after = (x.shape[:dim], x.shape[dim + 1 :])
    return jnp.moveaxis(x.reshape(*before, size, -1, *after), dim, 0)


def sum_at_owner(x, axis, dim):
    size = lax.axis_size(axis)
    tiles = lax.all_to_all(cut_along(x, dim, size), axis, 0, 0, tiled=True)
    return jnp.sum(tiles.astype(jnp.float32), axis=0)


def laid_out(tiles, dim):
    tiles = jnp.moveaxis(tiles, 0, dim)
    lengths = tiles.shape
    return tiles.reshape(*lengths[:dim], lengths[dim] * lengths[dim + 1], *lengths[dim + 2 :])


def copy_for_each(x, axis):
    size = lax.axis_size(axis)
    return lax.all_to_all(jnp.broadcast_to(x[None], (size, *x.shape)), axis, 0, 0, tiled=True)


def gathered_copies(x, axis, dim):
    return laid_out(copy_for_each(x, axis), dim)


def gather_turned(arrays, axis, dims):
    turned = [jnp.moveaxis(a, dim, 0) for a, dim in zip(arrays, dims)]
    both = jnp.concatenate([t.reshape(len(t), -1) for t in turned], axis=1)
    filled, at, done = (lax.all_gather(both, axis, axis=0, tiled=True), 0, [])
    for t, dim in zip(turned, dims):
        slab = filled[:, at : at + t[0].size].reshape(-1, *t.shape[1:])
        done.append(jnp.moveaxis(slab, 0, dim))
        at += t[0].size
    return tuple(done)


def contract_rows(left, right, precise):
    if precise:
        return lax.dot_general(
            left,
            right,
            (((0,), (0,)), ((), ())),
            precision=lax.Precision.HIGHEST,
            preferred_element_type=jnp.float32,
        )
    return lax.dot_general(
        left, right, (((0,), (0,)), ((), ())), preferred_element_type=jnp.float32
    )


def local(
    inputs,
    value_cotangent,
    first_map,
    second_map,
    lambdas,
    head_gain,
    output_cotangent,
    value_factor,
    output_factor,
    value_weight,
    output_weight,
    value_moment,
    value_second,
    output_moment,
    output_second,
):
    tok_rows = inputs.shape[0]
    local_heads = lambdas.shape[0]
    head_width = head_gain.shape[0]
    head_cols = local_heads * head_width
    first = first_map.astype(jnp.float32).reshape(tok_rows, local_heads, head_width)
    second = second_map.astype(jnp.float32).reshape(tok_rows, local_heads, head_width)
    difference = first - lambdas[None, :, None] * second
    normed = (
        difference
        * lax.rsqrt(jnp.mean(difference * difference, axis=-1, keepdims=True) + 1e-06)
        * head_gain
    )
    heads_out = normed.reshape(tok_rows, head_cols).astype(jnp.bfloat16)
    full_inputs, full_cotangent = side_by_side((inputs, output_cotangent), "tp", 1, 0)
    token_scale = 1.0 / math.sqrt(tok_rows * lax.axis_size("fs"))
    fs_index = lax.axis_index("fs")
    width_rows = value_weight.shape[0]
    value_rows = lax.dynamic_slice_in_dim(
        value_factor, fs_index * width_rows, width_rows, 0
    ).astype(jnp.float32)
    output_rows = lax.dynamic_slice_in_dim(
        output_factor, fs_index * width_rows, width_rows, 0
    ).astype(jnp.float32)
    grad_value = contract_rows(full_inputs, value_cotangent, False) * token_scale
    grad_output = contract_rows(full_cotangent, heads_out, False) * token_scale
    partial_value = jnp.concatenate(
        [
            contract_rows(value_factor.astype(jnp.float32), grad_value, True),
            contract_rows(output_factor.astype(jnp.float32), grad_output, True),
        ],
        axis=1,
    )
    own_rows = sum_at_owner(partial_value.astype(jnp.bfloat16), "fs", 0)
    moments = jnp.concatenate([value_moment, output_moment], axis=1)
    seconds = jnp.concatenate([value_second, output_second], axis=1)
    moment_new = 0.8 * moments + 0.2 * own_rows
    second_new = 0.95 * seconds + 0.05 * own_rows * own_rows
    direction = moment_new / (jnp.sqrt(second_new) + 1e-08)
    full_direction = gathered_copies(direction, "fs", 0)
    step_value = jnp.dot(
        value_rows,
        full_direction[:, :head_cols],
        precision=lax.Precision.HIGHEST,
        preferred_element_type=jnp.float32,
    )
    step_output = jnp.dot(
        output_rows,
        full_direction[:, head_cols:],
        precision=lax.Precision.HIGHEST,
        preferred_element_type=jnp.float32,
    )
    value_master = value_weight - 0.05 * step_value
    output_master = output_weight - 0.05 * step_output.T
    value_copy, output_copy = gather_turned(
        (value_master.astype(jnp.bfloat16), output_master.astype(jnp.bfloat16)), "fs", (0, 1)
    )
    return (
        value_master,
        output_master,
        moment_new[:, :head_cols],
        second_new[:, :head_cols],
        moment_new[:, head_cols:],
        second_new[:, head_cols:],
        value_copy,
        output_copy,
    )


def solution(mesh):
    in_specs = (
        P("fs", "tp"),
        P("fs", "tp"),
        P("fs", "tp"),
        P("fs", "tp"),
        P("tp"),
        P(),
        P("fs", "tp"),
        P(),
        P(),
        P("fs", "tp"),
        P("tp", "fs"),
        P("fs", "tp"),
        P("fs", "tp"),
        P("fs", "tp"),
        P("fs", "tp"),
    )
    out_specs = (
        P("fs", "tp"),
        P("tp", "fs"),
        P("fs", "tp"),
        P("fs", "tp"),
        P("fs", "tp"),
        P("fs", "tp"),
        P(None, "tp"),
        P("tp", None),
    )
    return jax.shard_map(local, mesh=mesh, in_specs=in_specs, out_specs=out_specs, check_vma=False)
```

profile of v0, /device:TPU:2, one launch (start us, length us, event | category | flops | bytes accessed | tf_op | source)
XLA Modules:
  0.0 207.0 jit_solution(13290908280082833347)
XLA Ops:
  7.2 0.0 copy-start
  7.2 0.0 copy-start.3
  7.2 0.0 copy-start.11
  7.2 0.0 copy-start.12
  7.2 0.0 all-gather.3.cloned.1.call-start
  7.3 1.9 pad_maximum_fusion
  9.2 0.0 all-gather.3.cloned.1.call-update
  9.2 0.0 copy-start.2
  9.2 1.3 reshape.84
  10.5 0.0 copy-done.3
  10.5 0.3 reshape.85
  10.8 0.7 multiply_reduce_fusion
  11.5 0.1 broadcast_bitcast_fusion
  11.6 44.3 %all-gather.3.cloned.1.call-done = bf16[1024,2048]{1,0:T(8,128)(2,1)} async-done(((bf16[1024,256]{1,0:T(8,128)(2,1)}), bf16[1024,2048]{1,0:T(8,128)(2,1)}) %all-gather.3.cloned.1.call-update) | async-done | bytes 4194320 | tf_op jit(solution)/shard_map/all_gather | solution.py:14
  55.9 0.6 mul.124
  56.5 0.0 copy-done.2
  56.6 0.0 copy-start.1
  56.6 2.5 %convolution_multiply_fusion = f32[2048,256]{1,0:T(8,128)S(1)} fusion(bf16[1024,2048]{1,0:T(8,128)(2,1)} %all-gather.3.cloned.1.call-done, f32[64,8,2,128]{3,2,1,0:T(2,128)S(1)} %bitcast.25, f32[256]{0:T(256)S(1)} %get-tuple-element.43, f32[256]{0:T(256)S(1)} %get-tuple-element.44, bf16[512,256]{1,0:T(8,128)(2,1)S(1)} %copy-done.3, ...), kind=kOutput, calls=%fused_computation | convolution fusion | flops 538312704 | bytes 5244928 | tf_op jit(solution)/shard_map/dot_general | solution.py:63
  59.1 0.0 copy-start.13
  59.1 1.5 fusion.3
  60.7 0.0 copy-done.13
  60.7 2.3 %convolution_multiply_fusion.1 = f32[2048,256]{1,0:T(8,128)S(1)} fusion(bf16[512,256]{1,0:T(8,128)(2,1)S(1)} %copy-done.13, bf16[1024,2048]{1,0:T(8,128)(2,1)} %all-gather.3.cloned.1.call-done), kind=kOutput, calls=%fused_computation.1 | convolution fusion | flops 537395200 | bytes 4456448 | tf_op jit(solution)/shard_map/dot_general | solution.py:63
  63.0 0.0 copy-start.7
  63.0 0.0 copy-start.8
  63.1 0.0 copy-start.9
  63.1 0.0 copy-start.10
  63.1 1.5 fusion.2
  64.6 0.0 copy-start.5
  64.6 0.0 copy-start.6
  64.6 0.1 pad_maximum_fusion.1
  64.8 28.4 %all_to_all.10 = bf16[64,4,512]{2,1,0:T(4,128)(2,1)S(1)} all-to-all(bf16[64,4,512]{2,1,0:T(4,128)(2,1)S(1)} %pad_maximum_fusion.1), channel_id=1, replica_groups=mesh['fs'=64,'tp'=8] {'fs'}, dimensions={0} | all-to-all | bytes 524288 | tf_op jit(solution)/shard_map/all_to_all | solution.py:24
  93.2 0.1 convert_reduce_fusion
  93.3 0.0 copy-done.8
  93.4 0.9 broadcast_in_dim.2
  94.3 4.6 %all-to-all-start.1 = ((f32[64,4,512]{2,1,0:T(4,128)}), f32[64,4,512]{2,1,0:T(4,128)S(1)}, u32[]{:S(2)}, u32[]{:S(2)}) async-start(f32[64,4,512]{2,1,0:T(4,128)} %broadcast_in_dim.2), calls=%async_computation.1 | async-start | bytes 1048576 | tf_op jit(solution)/shard_map/all_to_all | solution.py:36
  98.9 0.0 all-gather.5.cloned.1.call-start
  98.9 18.6 %all-to-all-done.1 = f32[64,4,512]{2,1,0:T(4,128)S(1)} async-done(((f32[64,4,512]{2,1,0:T(4,128)}), f32[64,4,512]{2,1,0:T(4,128)S(1)}, u32[]{:S(2)}, u32[]{:S(2)}) %all-to-all-start.1) | async-done | bytes 524320 | tf_op jit(solution)/shard_map/all_to_all | solution.py:36
  117.5 0.2 reshape.86
  117.7 0.2 fusion.4
  118.0 0.0 copy-start.4
  118.0 0.9 fusion.25
  118.9 0.6 pad_maximum_fusion.2
  119.5 0.0 all-gather.5.cloned.1.call-update
  119.5 0.6 fusion.23
  120.1 0.6 fusion.24
  120.7 75.4 %all-gather.5.cloned.1.call-done = bf16[2048,512]{1,0:T(8,128)(2,1)} async-done(((bf16[32,512]{1,0:T(8,128)(2,1)}), bf16[2048,512]{1,0:T(8,128)(2,1)}) %all-gather.5.cloned.1.call-update) | async-done | bytes 2097168 | tf_op jit(solution)/shard_map/all_gather | solution.py:46
  196.1 2.6 %slice_bitcast_fusion = (bf16[256,2048]{0,1:T(8,128)(2,1)S(1)}, bf16[2048,256]{1,0:T(8,128)(2,1)}) fusion(bf16[2048,512]{1,0:T(8,128)(2,1)} %all-gather.5.cloned.1.call-done), kind=kLoop, calls=%fused_computation.12 | loop fusion | bytes 4194304 | tf_op jit(solution)/shard_map/transpose | solution.py:49
  198.8 1.4 copy.28
  (15 shorter events, 0.2 us)
Async XLA Ops:
  7.2 55.9 %copy-start = (bf16[2048,256]{1,0:T(8,128)(2,1)S(1)}, bf16[2048,256]{1,0:T(8,128)(2,1)}, u32[]{:S(2)}) copy-start(bf16[2048,256]{1,0:T(8,128)(2,1)} %param.22) | copy-start | bytes 3145732
  7.2 3.3 %copy-start.3 = (bf16[512,256]{1,0:T(8,128)(2,1)S(1)}, bf16[512,256]{1,0:T(8,128)(2,1)}, u32[]{:S(2)}) copy-start(bf16[512,256]{1,0:T(8,128)(2,1)} %param.18) | copy-start | bytes 786436
  7.2 3.6 %copy-start.11 = (f32[2]{0:T(128)S(1)}, f32[2]{0:T(128)}, u32[]{:S(2)}) copy-start(f32[2]{0:T(128)} %param.19) | copy-start | bytes 28
  7.2 4.3 %copy-start.12 = (f32[128]{0:T(128)S(1)}, f32[128]{0:T(128)}, u32[]{:S(2)}) copy-start(f32[128]{0:T(128)} %param.20) | copy-start | bytes 1540
  7.2 48.7 %all-gather.3.cloned.1.call-start = ((), (), s32[]{:S(2)}) async-start(), calls=%async_computation.2 | async-start | bytes 4718592 | tf_op jit(solution)/shard_map/all_gather | solution.py:14
  9.2 47.3 %copy-start.2 = (bf16[512,256]{1,0:T(8,128)(2,1)S(1)}, bf16[512,256]{1,0:T(8,128)(2,1)}, u32[]{:S(2)}) copy-start(bf16[512,256]{1,0:T(8,128)(2,1)} %param.17) | copy-start | bytes 786436
  56.6 2.5 %copy-start.1 = (bf16[2048,256]{1,0:T(8,128)(2,1)S(1)}, bf16[2048,256]{1,0:T(8,128)(2,1)}, u32[]{:S(2)}) copy-start(bf16[2048,256]{1,0:T(8,128)(2,1)} %param.23) | copy-start | bytes 3145732
  59.1 1.6 copy-start.13
  63.0 30.3 %copy-start.7 = (f32[4,256]{1,0:T(4,128)S(1)}, f32[4,256]{1,0:T(4,128)}, u32[]{:S(2)}) copy-start(f32[4,256]{1,0:T(4,128)} %param.29) | copy-start | bytes 12292
  63.0 30.3 %copy-start.8 = (f32[4,256]{1,0:T(4,128)S(1)}, f32[4,256]{1,0:T(4,128)}, u32[]{:S(2)}) copy-start(f32[4,256]{1,0:T(4,128)} %param.27) | copy-start | bytes 12292
  63.1 30.3 %copy-start.9 = (f32[4,256]{1,0:T(4,128)S(1)}, f32[4,256]{1,0:T(4,128)}, u32[]{:S(2)}) copy-start(f32[4,256]{1,0:T(4,128)} %param.28) | copy-start | bytes 12292
  63.1 30.3 %copy-start.10 = (f32[4,256]{1,0:T(4,128)S(1)}, f32[4,256]{1,0:T(4,128)}, u32[]{:S(2)}) copy-start(f32[4,256]{1,0:T(4,128)} %param.26) | copy-start | bytes 12292
  64.6 53.2 %copy-start.5 = (f32[256,32]{0,1:T(8,128)S(1)}, f32[256,32]{0,1:T(8,128)}, u32[]{:S(2)}) copy-start(f32[256,32]{0,1:T(8,128)} %param.25) | copy-start | bytes 98308
  64.6 53.4 %copy-start.6 = (f32[32,256]{1,0:T(8,128)S(1)}, f32[32,256]{1,0:T(8,128)}, u32[]{:S(2)}) copy-start(f32[32,256]{1,0:T(8,128)} %param.24) | copy-start | bytes 98308
  94.3 23.3 %all-to-all-start.1 = ((f32[64,4,512]{2,1,0:T(4,128)}), f32[64,4,512]{2,1,0:T(4,128)S(1)}, u32[]{:S(2)}, u32[]{:S(2)}) async-start(f32[64,4,512]{2,1,0:T(4,128)} %broadcast_in_dim.2), calls=%async_computation.1 | async-start | bytes 1048576 | tf_op jit(solution)/shard_map/all_to_all | solution.py:36
  98.9 97.2 %all-gather.5.cloned.1.call-start = ((), (), s32[]{:S(2)}) async-start(), calls=%async_computation.3 | async-start | bytes 2129920 | tf_op jit(solution)/shard_map/all_gather | solution.py:46
  118.0 80.8 %copy-start.4 = (f32[256,32]{0,1:T(8,128)}, f32[256,32]{0,1:T(8,128)S(1)}, u32[]{:S(2)}) copy-start(f32[256,32]{0,1:T(8,128)S(1)} %fusion.4) | copy-start | bytes 98308
Sparse Core Ops, SparseCore 0:
  10.7 45.1 all-gather.2
  119.6 76.4 all-gather.4
where the time goes:
time: 207 us
  waiting for transfers between devices  138 us (67%)
  blocking collectives  28.4 us (14%)
  between operations  14.3 us (7%)
  matrix products  8.94 us (4%)
  local copies, waits for them, and re-layouts  8.65 us (4%)
  starting transfers between devices  4.71 us (2%)
  other arithmetic  3.6 us (2%)
    all_gather x1, waiting for transfers between devices, gather_turned(): filled, at, done = (lax.all_gather(both, axis, axis=0, tiled=True), 0, [])  75.4 us
    all_gather x1, waiting for transfers between devices, side_by_side(): lax.all_gather(both, axis, axis=dim, tiled=True)  44.3 us
    all_to_all x1, blocking collectives, sum_at_owner(): tiles = lax.all_to_all(cut_along(x, dim, size), axis, 0, 0, tiled=True)  28.4 us
    all_to_all x1, waiting for transfers between devices, copy_for_each(): lax.all_to_all(jnp.broadcast_to(x[None], (size, *x.shape)), axis, 0, 0, t...  18.6 us
    dot_general x2, matrix products, contract_rows(): lax.dot_general(left, right, (((0,), (0,)), ((), ())), preferred_element_...  4.85 us
    all_to_all x1, starting transfers between devices, copy_for_each(): lax.all_to_all(jnp.broadcast_to(x[None], (size, *x.shape)), axis, 0, 0, t...  4.63 us
  transfers between devices with their start and end apart: 3, of which 3 were waited for; matrix products, arithmetic and copies ran while one was open for 2% of the time, Pallas kernels for 0%

commit v1 on v0

--- a/solution.py
+++ b/solution.py
@@ -43,7 +43,13 @@
 def gather_turned(arrays, axis, dims):
     turned = [jnp.moveaxis(a, dim, 0) for a, dim in zip(arrays, dims)]
     both = jnp.concatenate([t.reshape(len(t), -1) for t in turned], axis=1)
-    filled, at, done = (lax.all_gather(both, axis, axis=0, tiled=True), 0, [])
+    filled, at, done = (
+        jnp.concatenate(
+            lax.all_to_all(jnp.stack([both] * lax.axis_size(axis)), axis, 0, 0), axis=0
+        ),
+        0,
+        [],
+    )
     for t, dim in zip(turned, dims):
         slab = filled[:, at : at + t[0].size].reshape(-1, *t.shape[1:])
         done.append(jnp.moveaxis(slab, 0, dim))

time: 207 us -> 188 us (0.908)
  waiting for transfers between devices: 138 us -> 113 us
  starting transfers between devices: 4.71 us -> 9.63 us
    all_gather x1 -> x0, waiting for transfers between devices: 75.4 us -> none  [gather_turned(): filled, at, done = (lax.all_gather(both, axis, axis=0, tiled=True), 0, [])]
    all_to_all x0 -> x1, waiting for transfers between devices: none -> 50.3 us  [gather_turned(): lax.all_to_all(jnp.stack([both] * lax.axis_size(axis)), axis, 0, 0)]
    all_to_all x0 -> x1, starting transfers between devices: none -> 4.96 us  [gather_turned(): lax.all_to_all(jnp.stack([both] * lax.axis_size(axis)), axis, 0, 0)]
where the time goes in v1:
time: 188 us
  waiting for transfers between devices  113 us (60%)
  blocking collectives  28.4 us (15%)
  between operations  14.3 us (8%)
  local copies, waits for them, and re-layouts  9.89 us (5%)
  starting transfers between devices  9.63 us (5%)
  matrix products  8.94 us (5%)
  other arithmetic  2.99 us (2%)
    all_to_all x1, waiting for transfers between devices, gather_turned(): lax.all_to_all(jnp.stack([both] * lax.axis_size(axis)), axis, 0, 0)  50.3 us
    all_gather x1, waiting for transfers between devices, side_by_side(): lax.all_gather(both, axis, axis=dim, tiled=True)  44.3 us
    all_to_all x1, blocking collectives, sum_at_owner(): tiles = lax.all_to_all(cut_along(x, dim, size), axis, 0, 0, tiled=True)  28.4 us
    all_to_all x1, waiting for transfers between devices, copy_for_each(): lax.all_to_all(jnp.broadcast_to(x[None], (size, *x.shape)), axis, 0, 0, t...  18.6 us
    all_to_all x1, starting transfers between devices, gather_turned(): lax.all_to_all(jnp.stack([both] * lax.axis_size(axis)), axis, 0, 0)  4.96 us
    dot_general x2, matrix products, contract_rows(): lax.dot_general(left, right, (((0,), (0,)), ((), ())), preferred_element_...  4.85 us
    all_to_all x1, starting transfers between devices, copy_for_each(): lax.all_to_all(jnp.broadcast_to(x[None], (size, *x.shape)), axis, 0, 0, t...  4.63 us
  transfers between devices with their start and end apart: 3, of which 3 were waited for; matrix products, arithmetic and copies ran while one was open for 2% of the time, Pallas kernels for 0%

profile of v1, /device:TPU:2, one launch (start us, length us, event | category | flops | bytes accessed | tf_op | source)
XLA Modules:
  0.0 187.5 jit_solution(9494529313948475233)
XLA Ops:
  7.2 0.0 copy-start
  7.2 0.0 copy-start.3
  7.2 0.0 copy-start.11
  7.2 0.0 copy-start.12
  7.2 0.0 all-gather.2.cloned.1.call-start
  7.3 1.9 %pad_maximum_fusion = bf16[1024,256]{1,0:T(8,128)(2,1)} fusion(bf16[512,256]{1,0:T(8,128)(2,1)} %param.21, bf16[512,256]{1,0:T(8,128)(2,1)} %param.15), kind=kLoop, calls=%fused_computation.16 | loop fusion | flops 1048576 | bytes 1048576 | tf_op jit(solution)/shard_map/concatenate | solution.py:13
  9.2 0.0 all-gather.2.cloned.1.call-update
  9.2 0.0 copy-start.2
  9.2 1.3 reshape.89
  10.5 0.0 copy-done.3
  10.5 0.3 reshape.90
  10.8 0.0 copy-done.11
  10.8 0.7 multiply_reduce_fusion
  11.5 0.1 broadcast_bitcast_fusion
  11.6 44.3 %all-gather.2.cloned.1.call-done = bf16[1024,2048]{1,0:T(8,128)(2,1)} async-done(((bf16[1024,256]{1,0:T(8,128)(2,1)}), bf16[1024,2048]{1,0:T(8,128)(2,1)}) %all-gather.2.cloned.1.call-update) | async-done | bytes 4194320 | tf_op jit(solution)/shard_map/all_gather | solution.py:14
  55.9 0.6 mul.124
  56.5 0.0 copy-done.2
  56.6 0.0 copy-start.1
  56.6 2.5 %convolution_multiply_fusion = f32[2048,256]{1,0:T(8,128)S(1)} fusion(bf16[1024,2048]{1,0:T(8,128)(2,1)} %all-gather.2.cloned.1.call-done, f32[64,8,2,128]{3,2,1,0:T(2,128)S(1)} %bitcast.27, f32[256]{0:T(256)S(1)} %get-tuple-element.51, f32[256]{0:T(256)S(1)} %get-tuple-element.52, bf16[512,256]{1,0:T(8,128)(2,1)S(1)} %copy-done.3, ...), kind=kOutput, calls=%fused_computation | convolution fusion | flops 538312704 | bytes 5244928 | tf_op jit(solution)/shard_map/dot_general | solution.py:69
  59.1 0.0 copy-start.13
  59.1 1.5 fusion.3
  60.7 0.0 copy-done.13
  60.7 2.3 %convolution_multiply_fusion.1 = f32[2048,256]{1,0:T(8,128)S(1)} fusion(bf16[512,256]{1,0:T(8,128)(2,1)S(1)} %copy-done.13, bf16[1024,2048]{1,0:T(8,128)(2,1)} %all-gather.2.cloned.1.call-done), kind=kOutput, calls=%fused_computation.1 | convolution fusion | flops 537395200 | bytes 4456448 | tf_op jit(solution)/shard_map/dot_general | solution.py:69
  63.0 0.0 copy-start.7
  63.0 0.0 copy-start.8
  63.1 0.0 copy-start.9
  63.1 0.0 copy-start.10
  63.1 1.5 fusion.2
  64.6 0.0 copy-start.5
  64.6 0.0 copy-start.6
  64.6 0.1 pad_maximum_fusion.1
  64.8 28.4 %all_to_all.15 = bf16[64,4,512]{2,1,0:T(4,128)(2,1)S(1)} all-to-all(bf16[64,4,512]{2,1,0:T(4,128)(2,1)S(1)} %pad_maximum_fusion.1), channel_id=1, replica_groups=mesh['fs'=64,'tp'=8] {'fs'}, dimensions={0} | all-to-all | bytes 524288 | tf_op jit(solution)/shard_map/all_to_all | solution.py:24
  93.2 0.1 convert_reduce_fusion
  93.3 0.0 copy-done.8
  93.4 0.9 broadcast_in_dim.2
  94.3 4.6 %all-to-all-start.1 = ((f32[64,4,512]{2,1,0:T(4,128)}), f32[64,4,512]{2,1,0:T(4,128)S(1)}, u32[]{:S(2)}, u32[]{:S(2)}) async-start(f32[64,4,512]{2,1,0:T(4,128)} %broadcast_in_dim.2), calls=%async_computation.1 | async-start | bytes 1048576 | tf_op jit(solution)/shard_map/all_to_all | solution.py:36
  98.9 18.6 %all-to-all-done.1 = f32[64,4,512]{2,1,0:T(4,128)S(1)} async-done(((f32[64,4,512]{2,1,0:T(4,128)}), f32[64,4,512]{2,1,0:T(4,128)S(1)}, u32[]{:S(2)}, u32[]{:S(2)}) %all-to-all-start.1) | async-done | bytes 524320 | tf_op jit(solution)/shard_map/all_to_all | solution.py:36
  117.5 0.2 reshape.91
  117.7 0.2 fusion.4
  118.0 0.0 copy-start.4
  118.0 0.9 fusion.25
  118.9 1.6 stack.2
  120.5 5.0 %all-to-all-start.2 = ((bf16[64,32,512]{2,1,0:T(8,128)(2,1)}), bf16[64,32,512]{2,1,0:T(8,128)(2,1)S(1)}, u32[]{:S(2)}, u32[]{:S(2)}) async-start(bf16[64,32,512]{2,1,0:T(8,128)(2,1)} %stack.2), calls=%async_computation.2 | async-start | bytes 4194304 | tf_op jit(solution)/shard_map/all_to_all | solution.py:48
  125.4 0.6 fusion.23
  126.0 0.6 fusion.24
  126.6 50.3 %all-to-all-done.2 = bf16[64,32,512]{2,1,0:T(8,128)(2,1)S(1)} async-done(((bf16[64,32,512]{2,1,0:T(8,128)(2,1)}), bf16[64,32,512]{2,1,0:T(8,128)(2,1)S(1)}, u32[]{:S(2)}, u32[]{:S(2)}) %all-to-all-start.2) | async-done | bytes 2097184 | tf_op jit(solution)/shard_map/all_to_all | solution.py:48
  177.0 1.5 slice_bitcast_fusion
  178.4 2.3 %copy.30 = bf16[256,2048]{1,0:T(8,128)(2,1)} copy(bf16[256,2048]{0,1:T(8,128)(2,1)} %get-tuple-element.43) | data formatting | bytes 2097152
  (15 shorter events, 0.2 us)
Async XLA Ops:
  7.2 55.9 %copy-start = (bf16[2048,256]{1,0:T(8,128)(2,1)S(1)}, bf16[2048,256]{1,0:T(8,128)(2,1)}, u32[]{:S(2)}) copy-start(bf16[2048,256]{1,0:T(8,128)(2,1)} %param.22) | copy-start | bytes 3145732
  7.2 3.3 %copy-start.3 = (bf16[512,256]{1,0:T(8,128)(2,1)S(1)}, bf16[512,256]{1,0:T(8,128)(2,1)}, u32[]{:S(2)}) copy-start(bf16[512,256]{1,0:T(8,128)(2,1)} %param.18) | copy-start | bytes 786436
  7.2 3.6 %copy-start.11 = (f32[2]{0:T(128)S(1)}, f32[2]{0:T(128)}, u32[]{:S(2)}) copy-start(f32[2]{0:T(128)} %param.19) | copy-start | bytes 28
  7.2 4.3 %copy-start.12 = (f32[128]{0:T(128)S(1)}, f32[128]{0:T(128)}, u32[]{:S(2)}) copy-start(f32[128]{0:T(128)} %param.20) | copy-start | bytes 1540
  7.2 48.7 %all-gather.2.cloned.1.call-start = ((), (), s32[]{:S(2)}) async-start(), calls=%async_computation.3 | async-start | bytes 4718592 | tf_op jit(solution)/shard_map/all_gather | solution.py:14
  9.2 47.3 %copy-start.2 = (bf16[512,256]{1,0:T(8,128)(2,1)S(1)}, bf16[512,256]{1,0:T(8,128)(2,1)}, u32[]{:S(2)}) copy-start(bf16[512,256]{1,0:T(8,128)(2,1)} %param.17) | copy-start | bytes 786436
  56.6 2.5 %copy-start.1 = (bf16[2048,256]{1,0:T(8,128)(2,1)S(1)}, bf16[2048,256]{1,0:T(8,128)(2,1)}, u32[]{:S(2)}) copy-start(bf16[2048,256]{1,0:T(8,128)(2,1)} %param.23) | copy-start | bytes 3145732
  59.1 1.6 copy-start.13
  63.0 30.3 %copy-start.7 = (f32[4,256]{1,0:T(4,128)S(1)}, f32[4,256]{1,0:T(4,128)}, u32[]{:S(2)}) copy-start(f32[4,256]{1,0:T(4,128)} %param.29) | copy-start | bytes 12292
  63.0 30.3 %copy-start.8 = (f32[4,256]{1,0:T(4,128)S(1)}, f32[4,256]{1,0:T(4,128)}, u32[]{:S(2)}) copy-start(f32[4,256]{1,0:T(4,128)} %param.27) | copy-start | bytes 12292
  63.1 30.3 %copy-start.9 = (f32[4,256]{1,0:T(4,128)S(1)}, f32[4,256]{1,0:T(4,128)}, u32[]{:S(2)}) copy-start(f32[4,256]{1,0:T(4,128)} %param.28) | copy-start | bytes 12292
  63.1 30.3 %copy-start.10 = (f32[4,256]{1,0:T(4,128)S(1)}, f32[4,256]{1,0:T(4,128)}, u32[]{:S(2)}) copy-start(f32[4,256]{1,0:T(4,128)} %param.26) | copy-start | bytes 12292
  64.6 53.2 %copy-start.5 = (f32[256,32]{0,1:T(8,128)S(1)}, f32[256,32]{0,1:T(8,128)}, u32[]{:S(2)}) copy-start(f32[256,32]{0,1:T(8,128)} %param.25) | copy-start | bytes 98308
  64.6 53.4 %copy-start.6 = (f32[32,256]{1,0:T(8,128)S(1)}, f32[32,256]{1,0:T(8,128)}, u32[]{:S(2)}) copy-start(f32[32,256]{1,0:T(8,128)} %param.24) | copy-start | bytes 98308
  94.3 23.3 %all-to-all-start.1 = ((f32[64,4,512]{2,1,0:T(4,128)}), f32[64,4,512]{2,1,0:T(4,128)S(1)}, u32[]{:S(2)}, u32[]{:S(2)}) async-start(f32[64,4,512]{2,1,0:T(4,128)} %broadcast_in_dim.2), calls=%async_computation.1 | async-start | bytes 1048576 | tf_op jit(solution)/shard_map/all_to_all | solution.py:36
  118.0 2.5 %copy-start.4 = (f32[256,32]{0,1:T(8,128)}, f32[256,32]{0,1:T(8,128)S(1)}, u32[]{:S(2)}) copy-start(f32[256,32]{0,1:T(8,128)S(1)} %fusion.4) | copy-start | bytes 98308
  120.5 56.5 %all-to-all-start.2 = ((bf16[64,32,512]{2,1,0:T(8,128)(2,1)}), bf16[64,32,512]{2,1,0:T(8,128)(2,1)S(1)}, u32[]{:S(2)}, u32[]{:S(2)}) async-start(bf16[64,32,512]{2,1,0:T(8,128)(2,1)} %stack.2), calls=%async_computation.2 | async-start | bytes 4194304 | tf_op jit(solution)/shard_map/all_to_all | solution.py:48
Sparse Core Ops, SparseCore 0:
  10.7 45.1 all-gather.1
